TPU v7x, 32 devices: a whole 2x2x4 slice. The times are simulated.
32 devices in a mesh: sp: 16 (over z, y, core), tp: 2 (over x).
Axes of the slice: x: 2, y: 2, z: 4, core: 2. Of those that a mesh axis runs over, the one named last changes fastest.
Arguments:
- queries: bfloat16 [3072, 1024], P('sp', 'tp'), may hold values from -6 to 6
- keys: bfloat16 [3072, 512], P('sp', 'tp'), may hold values from -6 to 6
- values: bfloat16 [3072, 512], P('sp', 'tp'), may hold values from -6 to 6
- q_gain: float32 [64], replicated, may hold values from 0.1 to 6.5
- k_gain: float32 [64], replicated, may hold values from 0.1 to 6.5
- w_out: bfloat16 [1024, 2048], P('tp'), may hold values from -12 to 12
- residual: bfloat16 [3072, 2048], P(('sp', 'tp')), may hold values from -6 to 6
- norm_gain: float32 [2048], replicated, may hold values from 0.1 to 1.9
- w_gate: bfloat16 [2048, 5632], P('sp', 'tp'), may hold values from -0.125 to 0.125
- w_up: bfloat16 [2048, 5632], P('sp', 'tp'), may hold values from -0.125 to 0.125
- w_down: bfloat16 [5632, 2048], P('tp', 'sp'), may hold values from -0.25 to 0.25
Outputs:
- layer_out: bfloat16 [3072, 2048], P(('sp', 'tp'))
All inputs are finite; a program needn't handle non-finite values.
Results may differ from a plain program's by a relative error of at most 0.018.
The roundings to bfloat16 on the way count: a program that leaves them out, or rounds other values in their place, can miss the bound.
Values may be sent and summed in bfloat16 or wider, within the bound.
A program may use at most 128 MiB of HBM per device.

v0:
```python
import math
import jax
import jax.numpy as jnp
from jax import lax
from jax.sharding import PartitionSpec as P

GRID_W = 128
EPS = 1e-06
THETA = 10000.0


def turn_half(part, angle):
    quarter = part.shape[-1] // 2
    cos_table = jnp.cos(angle)[:, None, :]
    sin_table = jnp.sin(angle)[:, None, :]
    first_part = part[..., :quarter]
    second_part = part[..., quarter:]
    return jnp.concatenate(
        [
            first_part * cos_table - second_part * sin_table,
            first_part * sin_table + second_part * cos_table,
        ],
        axis=-1,
    )


def head_norm_rope(flat, gain, offset, head_count):
    tok_rows = flat.shape[0]
    head_size = flat.shape[1] // head_count
    heads = flat.astype(jnp.float32).reshape(tok_rows, head_count, head_size)
    heads = heads * lax.rsqrt(jnp.mean(heads * heads, axis=-1, keepdims=True) + EPS) * gain
    positions = offset + jnp.arange(tok_rows, dtype=jnp.int32)
    row_pos = (positions // GRID_W).astype(jnp.float32)
    col_pos = (positions % GRID_W).astype(jnp.float32)
    half_size = head_size // 2
    inv_freq = THETA ** (-jnp.arange(0, half_size, 2, dtype=jnp.float32) / half_size)
    turned = jnp.concatenate(
        [
            turn_half(heads[..., :half_size], row_pos[:, None] * inv_freq[None, :]),
            turn_half(heads[..., half_size:], col_pos[:, None] * inv_freq[None, :]),
        ],
        axis=-1,
    )
    return turned.reshape(tok_rows, head_count * head_size).astype(jnp.bfloat16)


def body(queries, keys, values, q_gain, k_gain, w_out, residual, norm_gain, w_gate, w_up, w_down):
    tok_rows = queries.shape[0]
    head_size = q_gain.shape[0]
    q_heads = queries.shape[1] // head_size
    kv_heads = keys.shape[1] // head_size
    q_group = q_heads // kv_heads
    offset = lax.axis_index("sp") * tok_rows
    q_rot = head_norm_rope(queries, q_gain, offset, q_heads)
    k_rot = head_norm_rope(keys, k_gain, offset, kv_heads)
    query_groups = q_rot.reshape(tok_rows, kv_heads, q_group, head_size)
    score_scale = head_size ** (-0.5)
    start_state = (
        jnp.full((kv_heads, q_group, tok_rows), -1e30, jnp.float32),
        jnp.zeros((kv_heads, q_group, tok_rows), jnp.float32),
        jnp.zeros((kv_heads, q_group, tok_rows, head_size), jnp.float32),
    )
    running = start_state
    key_piece = lax.all_gather(k_rot, "sp", axis=0, tiled=True)
    value_piece = lax.all_gather(values, "sp", axis=0, tiled=True)
    piece_len = key_piece.shape[0]
    block_len = math.gcd(piece_len, 512)
    blocks = piece_len // block_len
    key_blocks = key_piece.reshape(blocks, block_len, kv_heads, head_size)
    value_blocks = value_piece.reshape(blocks, block_len, kv_heads, head_size)

    def update(state, block_pair):
        prior_max, totals, accum = state
        key_block, value_block = block_pair
        scores = (
            jnp.einsum(
                "qhgd,khd->hgqk", query_groups, key_block, preferred_element_type=jnp.float32
            )
            * score_scale
        )
        new_max = jnp.maximum(prior_max, jnp.max(scores, axis=-1))
        weights = jnp.exp(scores - new_max[..., None])
        factor = jnp.exp(prior_max - new_max)
        totals = totals * factor + jnp.sum(weights, axis=-1)
        accum = accum * factor[..., None] + jnp.einsum(
            "hgqk,khd->hgqd",
            weights.astype(jnp.bfloat16),
            value_block,
            preferred_element_type=jnp.float32,
        )
        return ((new_max, totals, accum), None)

    running, unused = lax.scan(update, running, (key_blocks, value_blocks))
    final_max, totals, accum = running
    mixed = accum / totals[..., None]
    attn = (
        jnp.transpose(mixed, (2, 0, 1, 3))
        .reshape(tok_rows, q_heads * head_size)
        .astype(jnp.bfloat16)
    )
    own_rows = lax.all_to_all(attn, "tp", split_axis=0, concat_axis=1, tiled=True)
    columns = own_rows
    proj = jnp.dot(
        columns, lax.all_gather(w_out, "tp", axis=0, tiled=True), preferred_element_type=jnp.float32
    )
    mid = residual.astype(jnp.float32) + proj
    normed = (
        mid * lax.rsqrt(jnp.mean(mid * mid, axis=-1, keepdims=True) + EPS) * norm_gain
    ).astype(jnp.bfloat16)
    gathered = lax.all_gather(normed, "tp", axis=0, tiled=True)
    columns = gathered
    gate = jnp.dot(
        columns,
        lax.all_gather(w_gate, "sp", axis=0, tiled=True),
        preferred_element_type=jnp.float32,
    )
    up_part = jnp.dot(
        columns, lax.all_gather(w_up, "sp", axis=0, tiled=True), preferred_element_type=jnp.float32
    )
    hidden = (jax.nn.silu(gate) * up_part).astype(jnp.bfloat16)
    terms = jnp.dot(
        hidden, lax.all_gather(w_down, "sp", axis=1, tiled=True), preferred_element_type=jnp.float32
    )
    down = lax.psum_scatter(
        terms.astype(jnp.bfloat16), "tp", scatter_dimension=0, tiled=True
    ).astype(jnp.float32)
    return (mid + 0.5 * down).astype(jnp.bfloat16)


def solution(mesh):
    return jax.shard_map(
        body,
        mesh=mesh,
        in_specs=(
            P("sp", "tp"),
            P("sp", "tp"),
            P("sp", "tp"),
            P(),
            P(),
            P("tp", None),
            P(("sp", "tp"), None),
            P(),
            P("sp", "tp"),
            P("sp", "tp"),
            P("tp", "sp"),
        ),
        out_specs=P(("sp", "tp"), None),
        check_vma=False,
    )
```

profile of v0, /device:TPU:0, one launch (start us, length us, event | category | flops | bytes accessed | tf_op | source)
XLA Modules:
  0.0 477.9 jit_solution(934830852998414411)
XLA Ops:
  6.6 1.0 copy.23
  7.7 0.7 fusion.24
  8.4 0.2 multiply_cosine_fusion.1
  8.7 0.7 copy.24
  9.5 0.7 all-gather.9.cloned.1.call-update
  10.3 0.7 all-gather.11.cloned.1.call-update
  11.0 0.5 all-gather.13.cloned.1.call-update
  11.6 0.5 all-gather.15.cloned.1.call-update
  12.2 0.5 all-gather.17.cloned.1.call-update
  12.8 0.1 copy.26
  12.9 0.1 fusion.21
  13.1 0.1 fusion.22
  13.2 0.1 subtract_convert_fusion.1
  13.3 38.7 %all-gather.7.cloned.1.call-done = bf16[3072,256]{1,0:T(8,128)(2,1)} async-done(((bf16[192,256]{1,0:T(8,128)(2,1)}), bf16[3072,256]{1,0:T(8,128)(2,1)}) %all-gather.7.cloned.1.call-update) | async-done | bytes 1572880 | tf_op jit(solution)/shard_map/all_gather | solution.py:64
  52.0 4.6 reshape.207
  56.6 3.3 copy.28
  59.9 32.7 %all-gather.9.cloned.1.call-done = bf16[3072,256]{1,0:T(8,128)(2,1)} async-done(((bf16[192,256]{1,0:T(8,128)(2,1)}), bf16[3072,256]{1,0:T(8,128)(2,1)}) %all-gather.9.cloned.1.call-update) | async-done | bytes 1572880 | tf_op jit(solution)/shard_map/all_gather | solution.py:65
  92.6 4.6 reshape.208
  97.2 3.3 copy.29
  100.5 32.2 %while.15 = (s32[]{:T(128)}, f32[4,2,192]{2,1,0:T(2,128)S(1)}, f32[4,2,192]{2,1,0:T(2,128)S(1)}, f32[4,2,192,64]{2,3,1,0:T(8,128)}, bf16[6,512,4,64]{1,3,2,0:T(8...) while((s32[]{:T(128)}, f32[4,2,192]{2,1,0:T(2,128)S(1)}, ...), condition=%wide.region_5.6_spmd.clone, body=%wide.region_2.5_spmd.clone.sunk | while | flops 207920640 | bytes 14189729 | solution.py:93
  100.5 1.7 bitcast_reduce_fusion.2
  102.3 0.9 fusion.50
  103.2 0.1 copy-done
  103.4 1.8 fusion.52
  105.2 0.8 copy-done.1
  106.0 1.7 bitcast_reduce_fusion.2
  107.7 0.9 fusion.50
  108.7 0.1 copy-done
  108.7 1.8 fusion.52
  110.5 0.8 copy-done.1
  111.4 1.7 bitcast_reduce_fusion.2
  113.1 0.9 fusion.50
  114.1 1.8 fusion.52
  115.9 0.8 copy-done.1
  116.7 1.7 bitcast_reduce_fusion.2
  118.4 0.9 fusion.50
  119.4 0.1 copy-done
  119.4 1.8 fusion.52
  121.3 0.8 copy-done.1
  122.1 1.7 bitcast_reduce_fusion.2
  123.8 0.9 fusion.50
  124.7 0.1 copy-done
  124.8 1.8 fusion.52
  126.6 0.8 copy-done.1
  127.4 1.7 bitcast_reduce_fusion.2
  129.1 0.9 fusion.50
  130.1 0.1 copy-done
  130.2 1.8 fusion.52
  132.0 0.8 copy-done.1
  132.8 1.1 fusion.25
  133.9 0.2 convert_element_type.65
  134.0 0.2 copy.30
  134.2 10.3 %all_to_all.16 = bf16[2,96,512]{2,1,0:T(8,128)(2,1)S(1)} all-to-all(bf16[2,96,512]{2,1,0:T(8,128)(2,1)S(1)} %copy.30), channel_id=1, replica_groups=mesh['sp'=16,'tp'=2] {'tp'}, dimensions={0} | all-to-all | bytes 393216 | tf_op jit(solution)/shard_map/all_to_all | solution.py:101
  144.5 7.2 %all-gather.11.cloned.1.call-done = bf16[1024,2048]{1,0:T(8,128)(2,1)} async-done(((bf16[512,2048]{1,0:T(8,128)(2,1)}), bf16[1024,2048]{1,0:T(8,128)(2,1)}) %all-gather.11.cloned.1.call-update) | async-done | bytes 4194320 | tf_op jit(solution)/shard_map/all_gather | solution.py:104
  151.7 3.2 multiply_reduce_fusion
  154.9 0.1 multiply_convert_fusion
  155.1 11.5 %all_gather.24 = bf16[192,2048]{1,0:T(8,128)(2,1)S(1)} all-gather(bf16[96,2048]{1,0:T(8,128)(2,1)S(1)} %multiply_convert_fusion), channel_id=1, replica_groups=mesh['sp'=16,'tp'=2] {'tp'}, dimensions={0}, use_global_device_ids=true | all-gather | bytes 1179648 | tf_op jit(solution)/shard_map/all_gather | solution.py:110
  166.6 81.3 %all-gather.13.cloned.1.call-done = bf16[2048,2816]{1,0:T(8,128)(2,1)} async-done(((bf16[128,2816]{1,0:T(8,128)(2,1)}), bf16[2048,2816]{1,0:T(8,128)(2,1)}) %all-gather.13.cloned.1.call-update) | async-done | bytes 11534352 | tf_op jit(solution)/shard_map/all_gather | solution.py:114
  247.9 8.0 %fusion.30 = f32[192,2816]{1,0:T(8,128)} fusion(bf16[192,2048]{1,0:T(8,128)(2,1)S(1)} %all_gather.24, bf16[2048,2816]{1,0:T(8,128)(2,1)} %all-gather.13.cloned.1.call-done), kind=kOutput, calls=%fused_computation.69 | convolution fusion | flops 2214592512 | bytes 14483456 | tf_op jit(solution)/shard_map/dot_general | solution.py:112
  255.9 86.4 %all-gather.15.cloned.1.call-done = bf16[2048,2816]{1,0:T(8,128)(2,1)} async-done(((bf16[128,2816]{1,0:T(8,128)(2,1)}), bf16[2048,2816]{1,0:T(8,128)(2,1)}) %all-gather.15.cloned.1.call-update) | async-done | bytes 11534352 | tf_op jit(solution)/shard_map/all_gather | solution.py:118
  342.3 97.2 %all-gather.17.cloned.1.call-done = bf16[2816,2048]{1,0:T(8,128)(2,1)} async-done(((bf16[2816,128]{1,0:T(8,128)(2,1)}), bf16[2816,2048]{1,0:T(8,128)(2,1)}) %all-gather.17.cloned.1.call-update) | async-done | bytes 11534352 | tf_op jit(solution)/shard_map/all_gather | solution.py:122
  439.4 13.9 %convolution_convert_fusion = bf16[192,2048]{1,0:T(8,128)(2,1)} fusion(bf16[2816,2048]{1,0:T(8,128)(2,1)} %all-gather.17.cloned.1.call-done, bf16[192,2048]{1,0:T(8,128)(2,1)S(1)} %all_gather.24, bf16[2048,2816]{1,0:T(8,128)(2,1)} %all-gather.15.cloned.1.call-done, f32[192,2816]{1,0:T(8,128)} %fusion.30), kind=kOutput, calls=%fused_computation.25 | convolution fusion | flops 4432822272 | bytes 26804224 | tf_op jit(solution)/shard_map/dot_general | solution.py:121
  453.3 15.8 %reduce-scatter.2.cloned.1.call-done = bf16[96,2048]{1,0:T(8,128)(2,1)} async-done(((bf16[192,2048]{1,0:T(8,128)(2,1)}), bf16[96,2048]{1,0:T(8,128)(2,1)}) %reduce-scatter.2.cloned.1.call-update) | async-done | bytes 393232 | tf_op jit(solution)/shard_map/reduce_scatter | solution.py:124
  469.2 1.8 add_convert_fusion
  (59 shorter events, 0.8 us)
Async XLA Ops:
  6.5 6.3 %copy-start.2 = (bf16[192,512]{1,0:T(8,128)(2,1)S(1)}, bf16[192,512]{1,0:T(8,128)(2,1)}, u32[]{:S(2)}) copy-start(bf16[192,512]{1,0:T(8,128)(2,1)} %param.13) | copy-start | bytes 589828
  6.5 45.4 %all-gather.7.cloned.1.call-start = ((), (), s32[]{:S(2)}) async-start(), calls=%async_computation.2 | async-start | bytes 1671168 | tf_op jit(solution)/shard_map/all_gather | solution.py:64
  8.4 4.6 copy-start.4
  9.5 83.1 %all-gather.9.cloned.1.call-start = ((), (), s32[]{:S(2)}) async-start(), calls=%async_computation.3 | async-start | bytes 1671168 | tf_op jit(solution)/shard_map/all_gather | solution.py:65
  10.2 141.5 %all-gather.11.cloned.1.call-start = ((), (), s32[]{:S(2)}) async-start(), calls=%async_computation.4 | async-start | bytes 6291456 | tf_op jit(solution)/shard_map/all_gather | solution.py:104
  11.0 236.9 %all-gather.13.cloned.1.call-start = ((), (), s32[]{:S(2)}) async-start(), calls=%async_computation.5 | async-start | bytes 12255232 | tf_op jit(solution)/shard_map/all_gather | solution.py:114
  11.6 330.7 %all-gather.15.cloned.1.call-start = ((), (), s32[]{:S(2)}) async-start(), calls=%async_computation.6 | async-start | bytes 12255232 | tf_op jit(solution)/shard_map/all_gather | solution.py:118
  12.1 427.3 %all-gather.17.cloned.1.call-start = ((), (), s32[]{:S(2)}) async-start(), calls=%async_computation.7 | async-start | bytes 12255232 | tf_op jit(solution)/shard_map/all_gather | solution.py:122
  12.7 456.4 %reduce-scatter.2.cloned.1.call-start = ((), (), s32[]{:S(2)}) async-start(), calls=%async_computation.8 | async-start | bytes 1179648 | tf_op jit(solution)/shard_map/reduce_scatter | solution.py:124
  102.3 1.1 copy-start
  105.2 0.8 copy-start.1
  107.7 1.0 copy-start
  110.5 0.8 copy-start.1
  113.0 1.0 copy-start
  115.9 0.8 copy-start.1
  118.4 1.0 copy-start
  121.2 0.8 copy-start.1
  123.8 1.0 copy-start
  126.6 0.8 copy-start.1
  129.1 1.0 copy-start
  132.0 0.8 copy-start.1
  134.2 20.7 %copy-start.3 = (f32[2048]{0:T(1024)S(1)}, f32[2048]{0:T(1024)}, u32[]{:S(2)}) copy-start(f32[2048]{0:T(1024)} %param.20) | copy-start | bytes 24580
Sparse Core Ops, SparseCore 0:
  9.6 42.3 all-gather.6
  54.3 38.2 all-gather.8
  94.1 57.5 all-gather.10
  153.9 93.9 all-gather.12
  250.0 92.2 all-gather.14
  344.3 95.1 all-gather.16
  453.4 15.6 reduce-scatter.1
where the time goes:
time: 479 us; the launch traced here: 478 us
  waiting for transfers between devices  362 us (76%)
  matrix products  46 us (10%)
  local copies, waits for them, and re-layouts  23.4 us (5%)
  blocking collectives  21.8 us (5%)
  between operations  13.7 us (3%)
  other arithmetic  10.2 us (2%)
    all_gather x1, waiting for transfers between devices, body(): lax.all_gather(w_down, 'sp', axis=1, tiled=True)  97.2 us
    all_gather x1, waiting for transfers between devices, body(): lax.all_gather(w_up, 'sp', axis=0, tiled=True)  86.4 us
    all_gather x1, waiting for transfers between devices, body(): lax.all_gather(w_gate, 'sp', axis=0, tiled=True)  81.3 us
    all_gather x1, waiting for transfers between devices, body(): key_piece = lax.all_gather(k_rot, 'sp', axis=0, tiled=True)  38.7 us
    all_gather x1, waiting for transfers between devices, body(): value_piece = lax.all_gather(values, 'sp', axis=0, tiled=True)  32.7 us
    reduce_scatter x1, waiting for transfers between devices, body(): lax.psum_scatter(terms.astype(jnp.bfloat16), 'tp', scatter_dimension=0, t...  15.8 us
    dot_general x1, matrix products, body(): jnp.dot(hidden, lax.all_gather(w_down, 'sp', axis=1, tiled=True), preferr...  13.9 us
    all_gather x1, blocking collectives, body(): gathered = lax.all_gather(normed, 'tp', axis=0, tiled=True)  11.5 us
  transfers between devices with their start and end apart: 7, of which 7 were waited for; matrix products, arithmetic and copies ran while one was open for 12% of the time, Pallas kernels for 0%

commit v1 on v0

--- a/solution.py
+++ b/solution.py
@@ -62,7 +62,12 @@
     )
     running = start_state
     key_piece = lax.all_gather(k_rot, "sp", axis=0, tiled=True)
-    value_piece = lax.all_gather(values, "sp", axis=0, tiled=True)
+    ring = [values]
+    for hop in range(15):
+        ring.append(lax.ppermute(ring[-1], "sp", [(dev, (dev + 1) % 16) for dev in range(16)]))
+    value_piece = jnp.roll(
+        jnp.concatenate(ring[::-1], axis=0), (lax.axis_index("sp") + 1) * ring[0].shape[0], axis=0
+    )
     piece_len = key_piece.shape[0]
     block_len = math.gcd(piece_len, 512)
     blocks = piece_len // block_len

time: 479 us -> 438 us (0.914)
  waiting for transfers between devices: 362 us -> 324 us
  blocking collectives: 21.8 us -> 16.2 us
    ppermute x0 -> x15, waiting for transfers between devices: none -> 103 us  [body(): lax.ppermute(ring[-1], 'sp', [(dev, (dev + 1) % 16) for dev in range(16)])]
    all_gather x1, waiting for transfers between devices: 81.3 us -> 18.9 us  [body(): lax.all_gather(w_gate, 'sp', axis=0, tiled=True)]
    all_gather x1, waiting for transfers between devices: 38.7 us -> 0.01 us  [body(): key_piece = lax.all_gather(k_rot, 'sp', axis=0, tiled=True)]
    all_gather x1 -> x0, waiting for transfers between devices: 32.7 us -> none  [body(): value_piece = lax.all_gather(values, 'sp', axis=0, tiled=True)]
    all_gather x1, waiting for transfers between devices: 7.22 us -> 0.02 us  [body(): lax.all_gather(w_out, 'tp', axis=0, tiled=True)]
  transfers between devices with their start and end apart: 7 -> 21, of which waited for: 7 -> 19; matrix products, arithmetic and copies ran while one was open for 12% -> 13% of each run, Pallas kernels for 0% -> 0%
where the time goes in v1:
time: 438 us; the launch traced here: 437 us
  waiting for transfers between devices  324 us (74%)
  matrix products  45.9 us (10%)
  local copies, waits for them, and re-layouts  25.3 us (6%)
  blocking collectives  16.2 us (4%)
  between operations  14 us (3%)
  other arithmetic  10.2 us (2%)
    ppermute x15, waiting for transfers between devices, body(): lax.ppermute(ring[-1], 'sp', [(dev, (dev + 1) % 16) for dev in range(16)])  103 us
    all_gather x1, waiting for transfers between devices, body(): lax.all_gather(w_down, 'sp', axis=1, tiled=True)  97.2 us
    all_gather x1, waiting for transfers between devices, body(): lax.all_gather(w_up, 'sp', axis=0, tiled=True)  86.4 us
    all_gather x1, waiting for transfers between devices, body(): lax.all_gather(w_gate, 'sp', axis=0, tiled=True)  18.9 us
    reduce_scatter x1, waiting for transfers between devices, body(): lax.psum_scatter(terms.astype(jnp.bfloat16), 'tp', scatter_dimension=0, t...  15.8 us
    dot_general x1, matrix products, body(): jnp.dot(hidden, lax.all_gather(w_down, 'sp', axis=1, tiled=True), preferr...  13.8 us
    dot_general x6, matrix products, update(): jnp.einsum('hgqk,khd->hgqd', weights.astype(jnp.bfloat16), value_block, p...  10.9 us
    dot_general x6, matrix products, update(): jnp.einsum('qhgd,khd->hgqk', query_groups, key_block, preferred_element_t...  10.1 us
  transfers between devices with their start and end apart: 21, of which 19 were waited for; matrix products, arithmetic and copies ran while one was open for 13% of the time, Pallas kernels for 0%

profile of v1, /device:TPU:0, one launch (start us, length us, event | category | flops | bytes accessed | tf_op | source)
XLA Modules:
  0.0 436.6 jit_solution(17746204949857592274)
XLA Ops:
  6.6 1.1 copy.23
  7.7 0.7 fusion.24
  8.7 0.7 copy.24
  9.6 0.7 all-gather.8.cloned.1.call-update
  10.3 0.7 all-gather.10.cloned.1.call-update
  11.0 0.5 all-gather.12.cloned.1.call-update
  11.6 0.5 all-gather.14.cloned.1.call-update
  12.2 0.5 collective-permute-start
  12.8 7.3 %collective-permute-done = bf16[192,256]{1,0:T(8,128)(2,1)S(1)} collective-permute-done((bf16[192,256]{1,0:T(8,128)(2,1)S(1)}, bf16[192,256]{1,0:T(8,128)(2,1)S(1)}, u32[]{:S(2)}, u32[]{:S(2)}) %collective-permute-start) | collective-permute-done | bytes 98336 | tf_op jit(solution)/shard_map/ppermute | solution.py:67
  20.0 7.8 %collective-permute-done.1 = bf16[192,256]{1,0:T(8,128)(2,1)S(1)} collective-permute-done((bf16[192,256]{1,0:T(8,128)(2,1)S(1)}, bf16[192,256]{1,0:T(8,128)(2,1)S(1)}, u32[]{:S(2)}, u32[]{:S(2)}) %collective-permute-start.1) | collective-permute-done | bytes 98336 | tf_op jit(solution)/shard_map/ppermute | solution.py:67
  27.9 6.9 %collective-permute-done.2 = bf16[192,256]{1,0:T(8,128)(2,1)S(1)} collective-permute-done((bf16[192,256]{1,0:T(8,128)(2,1)S(1)}, bf16[192,256]{1,0:T(8,128)(2,1)S(1)}, u32[]{:S(2)}, u32[]{:S(2)}) %collective-permute-start.2) | collective-permute-done | bytes 98336 | tf_op jit(solution)/shard_map/ppermute | solution.py:67
  34.8 6.9 %collective-permute-done.3 = bf16[192,256]{1,0:T(8,128)(2,1)S(1)} collective-permute-done((bf16[192,256]{1,0:T(8,128)(2,1)S(1)}, bf16[192,256]{1,0:T(8,128)(2,1)S(1)}, u32[]{:S(2)}, u32[]{:S(2)}) %collective-permute-start.3) | collective-permute-done | bytes 98336 | tf_op jit(solution)/shard_map/ppermute | solution.py:67
  41.7 7.4 %collective-permute-done.4 = bf16[192,256]{1,0:T(8,128)(2,1)S(1)} collective-permute-done((bf16[192,256]{1,0:T(8,128)(2,1)S(1)}, bf16[192,256]{1,0:T(8,128)(2,1)S(1)}, u32[]{:S(2)}, u32[]{:S(2)}) %collective-permute-start.4) | collective-permute-done | bytes 98336 | tf_op jit(solution)/shard_map/ppermute | solution.py:67
  49.1 6.7 %collective-permute-done.5 = bf16[192,256]{1,0:T(8,128)(2,1)S(1)} collective-permute-done((bf16[192,256]{1,0:T(8,128)(2,1)S(1)}, bf16[192,256]{1,0:T(8,128)(2,1)S(1)}, u32[]{:S(2)}, u32[]{:S(2)}) %collective-permute-start.5) | collective-permute-done | bytes 98336 | tf_op jit(solution)/shard_map/ppermute | solution.py:67
  55.8 6.7 %collective-permute-done.6 = bf16[192,256]{1,0:T(8,128)(2,1)S(1)} collective-permute-done((bf16[192,256]{1,0:T(8,128)(2,1)S(1)}, bf16[192,256]{1,0:T(8,128)(2,1)S(1)}, u32[]{:S(2)}, u32[]{:S(2)}) %collective-permute-start.6) | collective-permute-done | bytes 98336 | tf_op jit(solution)/shard_map/ppermute | solution.py:67
  62.6 6.7 %collective-permute-done.7 = bf16[192,256]{1,0:T(8,128)(2,1)S(1)} collective-permute-done((bf16[192,256]{1,0:T(8,128)(2,1)S(1)}, bf16[192,256]{1,0:T(8,128)(2,1)S(1)}, u32[]{:S(2)}, u32[]{:S(2)}) %collective-permute-start.7) | collective-permute-done | bytes 98336 | tf_op jit(solution)/shard_map/ppermute | solution.py:67
  69.3 6.7 %collective-permute-done.8 = bf16[192,256]{1,0:T(8,128)(2,1)S(1)} collective-permute-done((bf16[192,256]{1,0:T(8,128)(2,1)S(1)}, bf16[192,256]{1,0:T(8,128)(2,1)S(1)}, u32[]{:S(2)}, u32[]{:S(2)}) %collective-permute-start.8) | collective-permute-done | bytes 98336 | tf_op jit(solution)/shard_map/ppermute | solution.py:67
  76.2 6.6 %collective-permute-done.9 = bf16[192,256]{1,0:T(8,128)(2,1)S(1)} collective-permute-done((bf16[192,256]{1,0:T(8,128)(2,1)S(1)}, bf16[192,256]{1,0:T(8,128)(2,1)S(1)}, u32[]{:S(2)}, u32[]{:S(2)}) %collective-permute-start.9) | collective-permute-done | bytes 98336 | tf_op jit(solution)/shard_map/ppermute | solution.py:67
  82.9 6.7 %collective-permute-done.10 = bf16[192,256]{1,0:T(8,128)(2,1)S(1)} collective-permute-done((bf16[192,256]{1,0:T(8,128)(2,1)S(1)}, bf16[192,256]{1,0:T(8,128)(2,1)S(1)}, u32[]{:S(2)}, u32[]{:S(2)}) %collective-permute-start.10) | collective-permute-done | bytes 98336 | tf_op jit(solution)/shard_map/ppermute | solution.py:67
  89.6 6.7 %collective-permute-done.11 = bf16[192,256]{1,0:T(8,128)(2,1)S(1)} collective-permute-done((bf16[192,256]{1,0:T(8,128)(2,1)S(1)}, bf16[192,256]{1,0:T(8,128)(2,1)S(1)}, u32[]{:S(2)}, u32[]{:S(2)}) %collective-permute-start.11) | collective-permute-done | bytes 98336 | tf_op jit(solution)/shard_map/ppermute | solution.py:67
  96.4 6.6 %collective-permute-done.12 = bf16[192,256]{1,0:T(8,128)(2,1)S(1)} collective-permute-done((bf16[192,256]{1,0:T(8,128)(2,1)S(1)}, bf16[192,256]{1,0:T(8,128)(2,1)S(1)}, u32[]{:S(2)}, u32[]{:S(2)}) %collective-permute-start.12) | collective-permute-done | bytes 98336 | tf_op jit(solution)/shard_map/ppermute | solution.py:67
  103.2 6.6 %collective-permute-done.13 = bf16[192,256]{1,0:T(8,128)(2,1)S(1)} collective-permute-done((bf16[192,256]{1,0:T(8,128)(2,1)S(1)}, bf16[192,256]{1,0:T(8,128)(2,1)S(1)}, u32[]{:S(2)}, u32[]{:S(2)}) %collective-permute-start.13) | collective-permute-done | bytes 98336 | tf_op jit(solution)/shard_map/ppermute | solution.py:67
  109.8 6.7 %collective-permute-done.14 = bf16[192,256]{1,0:T(8,128)(2,1)S(1)} collective-permute-done((bf16[192,256]{1,0:T(8,128)(2,1)S(1)}, bf16[192,256]{1,0:T(8,128)(2,1)S(1)}, u32[]{:S(2)}, u32[]{:S(2)}) %collective-permute-start.14) | collective-permute-done | bytes 98336 | tf_op jit(solution)/shard_map/ppermute | solution.py:67
  117.0 1.6 constant_dynamic-slice_fusion
  118.6 4.6 %reshape.208 = bf16[6,512,4,64]{3,2,1,0:T(4,128)(2,1)S(1)} reshape(bf16[3072,256]{1,0:T(8,128)(2,1)} %constant_dynamic-slice_fusion) | data formatting | bytes 3145728 | tf_op jit(solution)/shard_map/reshape | solution.py:75
  123.2 3.3 copy.29
  126.6 4.6 %reshape.207 = bf16[6,512,4,64]{3,2,1,0:T(4,128)(2,1)S(1)} reshape(bf16[3072,256]{1,0:T(8,128)(2,1)} %all-gather.6.cloned.1.call-done) | data formatting | bytes 3145728 | tf_op jit(solution)/shard_map/reshape | solution.py:74
  131.2 3.3 copy.28
  134.5 32.2 %while.15 = (s32[]{:T(128)}, f32[4,2,192]{2,1,0:T(2,128)S(1)}, f32[4,2,192]{2,1,0:T(2,128)S(1)}, f32[4,2,192,64]{2,3,1,0:T(8,128)}, bf16[6,512,4,64]{1,3,2,0:T(8...) while((s32[]{:T(128)}, f32[4,2,192]{2,1,0:T(2,128)S(1)}, ...), condition=%wide.region_5.6_spmd.clone, body=%wide.region_2.5_spmd.clone.sunk | while | flops 207920640 | bytes 14189729 | solution.py:98
  134.5 1.7 bitcast_reduce_fusion.2
  136.2 0.9 fusion.50
  137.2 1.8 fusion.52
  139.1 0.8 copy-done.1
  139.8 1.7 bitcast_reduce_fusion.2
  141.6 0.9 fusion.50
  142.6 1.8 fusion.52
  144.4 0.8 copy-done.1
  145.2 1.7 bitcast_reduce_fusion.2
  146.9 0.9 fusion.50
  147.9 1.8 fusion.52
  149.7 0.8 copy-done.1
  150.5 1.7 bitcast_reduce_fusion.2
  152.2 0.9 fusion.50
  153.4 1.8 fusion.52
  155.3 0.8 copy-done.1
  156.1 1.7 bitcast_reduce_fusion.2
  157.8 0.9 fusion.50
  158.8 1.8 fusion.52
  160.6 0.8 copy-done.1
  161.4 1.7 bitcast_reduce_fusion.2
  163.1 0.9 fusion.50
  164.1 1.8 fusion.52
  166.0 0.8 copy-done.1
  166.8 1.1 fusion.25
  168.2 7.6 %all_to_all.16 = bf16[2,96,512]{2,1,0:T(8,128)(2,1)S(1)} all-to-all(bf16[2,96,512]{2,1,0:T(8,128)(2,1)S(1)} %copy.30), channel_id=1, replica_groups=mesh['sp'=16,'tp'=2] {'tp'}, dimensions={0} | all-to-all | bytes 393216 | tf_op jit(solution)/shard_map/all_to_all | solution.py:106
  175.8 3.2 multiply_reduce_fusion
  179.2 8.6 %all_gather.20 = bf16[192,2048]{1,0:T(8,128)(2,1)S(1)} all-gather(bf16[96,2048]{1,0:T(8,128)(2,1)S(1)} %multiply_convert_fusion), channel_id=1, replica_groups=mesh['sp'=16,'tp'=2] {'tp'}, dimensions={0}, use_global_device_ids=true | all-gather | bytes 1179648 | tf_op jit(solution)/shard_map/all_gather | solution.py:115
  187.8 18.9 %all-gather.10.cloned.1.call-done = bf16[2048,2816]{1,0:T(8,128)(2,1)} async-done(((bf16[128,2816]{1,0:T(8,128)(2,1)}), bf16[2048,2816]{1,0:T(8,128)(2,1)}) %all-gather.10.cloned.1.call-update) | async-done | bytes 11534352 | tf_op jit(solution)/shard_map/all_gather | solution.py:119
  206.7 8.0 %fusion.30 = f32[192,2816]{1,0:T(8,128)} fusion(bf16[192,2048]{1,0:T(8,128)(2,1)S(1)} %all_gather.20, bf16[2048,2816]{1,0:T(8,128)(2,1)} %all-gather.10.cloned.1.call-done), kind=kOutput, calls=%fused_computation.102 | convolution fusion | flops 2214592512 | bytes 14483456 | tf_op jit(solution)/shard_map/dot_general | solution.py:117
  214.7 86.4 %all-gather.12.cloned.1.call-done = bf16[2048,2816]{1,0:T(8,128)(2,1)} async-done(((bf16[128,2816]{1,0:T(8,128)(2,1)}), bf16[2048,2816]{1,0:T(8,128)(2,1)}) %all-gather.12.cloned.1.call-update) | async-done | bytes 11534352 | tf_op jit(solution)/shard_map/all_gather | solution.py:123
  301.1 97.2 %all-gather.14.cloned.1.call-done = bf16[2816,2048]{1,0:T(8,128)(2,1)} async-done(((bf16[2816,128]{1,0:T(8,128)(2,1)}), bf16[2816,2048]{1,0:T(8,128)(2,1)}) %all-gather.14.cloned.1.call-update) | async-done | bytes 11534352 | tf_op jit(solution)/shard_map/all_gather | solution.py:127
  398.3 13.8 %convolution_convert_fusion = bf16[192,2048]{1,0:T(8,128)(2,1)} fusion(bf16[2816,2048]{1,0:T(8,128)(2,1)} %all-gather.14.cloned.1.call-done, bf16[192,2048]{1,0:T(8,128)(2,1)S(1)} %all_gather.20, bf16[2048,2816]{1,0:T(8,128)(2,1)} %all-gather.12.cloned.1.call-done, f32[192,2816]{1,0:T(8,128)} %fusion.30), kind=kOutput, calls=%fused_computation.25 | convolution fusion | flops 4432822272 | bytes 26804224 | tf_op jit(solution)/shard_map/dot_general | solution.py:126
  412.1 15.8 %reduce-scatter.2.cloned.1.call-done = bf16[96,2048]{1,0:T(8,128)(2,1)} async-done(((bf16[192,2048]{1,0:T(8,128)(2,1)}), bf16[96,2048]{1,0:T(8,128)(2,1)}) %reduce-scatter.2.cloned.1.call-update) | async-done | bytes 393232 | tf_op jit(solution)/shard_map/reduce_scatter | solution.py:129
  427.9 1.8 add_convert_fusion
  (121 shorter events, 2.6 us)
Async XLA Ops:
  6.5 5.7 %copy-start.2 = (bf16[192,256]{1,0:T(8,128)(2,1)S(1)}, bf16[192,256]{1,0:T(8,128)(2,1)}, u32[]{:S(2)}) copy-start(bf16[192,256]{1,0:T(8,128)(2,1)} %param.15) | copy-start | bytes 294916
  6.5 69.5 %copy-start.3 = (bf16[192,512]{1,0:T(8,128)(2,1)S(1)}, bf16[192,512]{1,0:T(8,128)(2,1)}, u32[]{:S(2)}) copy-start(bf16[192,512]{1,0:T(8,128)(2,1)} %param.13) | copy-start | bytes 589828
  6.5 120.0 %all-gather.6.cloned.1.call-start = ((), (), s32[]{:S(2)}) async-start(), calls=%async_computation.2 | async-start | bytes 1671168 | tf_op jit(solution)/shard_map/all_gather | solution.py:64
  8.4 87.8 %copy-start.5 = (f32[64]{0:T(128)S(1)}, f32[64]{0:T(128)}, u32[]{:S(2)}) copy-start(f32[64]{0:T(128)} %param.16) | copy-start | bytes 772
  9.5 166.3 %all-gather.8.cloned.1.call-start = ((), (), s32[]{:S(2)}) async-start(), calls=%async_computation.3 | async-start | bytes 6291456 | tf_op jit(solution)/shard_map/all_gather | solution.py:109
  10.3 196.4 %all-gather.10.cloned.1.call-start = ((), (), s32[]{:S(2)}) async-start(), calls=%async_computation.4 | async-start | bytes 12255232 | tf_op jit(solution)/shard_map/all_gather | solution.py:119
  11.0 290.1 %all-gather.12.cloned.1.call-start = ((), (), s32[]{:S(2)}) async-start(), calls=%async_computation.5 | async-start | bytes 12255232 | tf_op jit(solution)/shard_map/all_gather | solution.py:123
  11.6 386.7 %all-gather.14.cloned.1.call-start = ((), (), s32[]{:S(2)}) async-start(), calls=%async_computation.6 | async-start | bytes 12255232 | tf_op jit(solution)/shard_map/all_gather | solution.py:127
  12.2 415.8 %reduce-scatter.2.cloned.1.call-start = ((), (), s32[]{:S(2)}) async-start(), calls=%async_computation.7 | async-start | bytes 1179648 | tf_op jit(solution)/shard_map/reduce_scatter | solution.py:129
  12.2 7.8 %collective-permute-start = (bf16[192,256]{1,0:T(8,128)(2,1)S(1)}, bf16[192,256]{1,0:T(8,128)(2,1)S(1)}, u32[]{:S(2)}, u32[]{:S(2)}) collective-permute-start(bf16[192,256]{1,0:T(8,128)(2,1)S(1)} %copy-done.2), channel_id=1, source_target_pairs={{0,2},{2,4},{4,6},{6,8},{8,10},{10,12},{12,14},{14,16},{16,18},{18... | collective-permute-start | bytes 294920 | tf_op jit(solution)/shard_map/ppermute | solution.py:67
  20.0 7.8 %collective-permute-start.1 = (bf16[192,256]{1,0:T(8,128)(2,1)S(1)}, bf16[192,256]{1,0:T(8,128)(2,1)S(1)}, u32[]{:S(2)}, u32[]{:S(2)}) collective-permute-start(bf16[192,256]{1,0:T(8,128)(2,1)S(1)} %collective-permute-done), channel_id=1, source_target_pairs={{0,2},{2,4},{4,6},{6,8},{8,10},{10,12},{12,14},{14,16},{16,18},{18... | collective-permute-start | bytes 294920 | tf_op jit(solution)/shard_map/ppermute | solution.py:67
  27.9 6.9 %collective-permute-start.2 = (bf16[192,256]{1,0:T(8,128)(2,1)S(1)}, bf16[192,256]{1,0:T(8,128)(2,1)S(1)}, u32[]{:S(2)}, u32[]{:S(2)}) collective-permute-start(bf16[192,256]{1,0:T(8,128)(2,1)S(1)} %collective-permute-done.1), channel_id=1, source_target_pairs={{0,2},{2,4},{4,6},{6,8},{8,10},{10,12},{12,14},{14,16},{16,18},{18... | collective-permute-start | bytes 294920 | tf_op jit(solution)/shard_map/ppermute | solution.py:67
  34.8 6.9 %collective-permute-start.3 = (bf16[192,256]{1,0:T(8,128)(2,1)S(1)}, bf16[192,256]{1,0:T(8,128)(2,1)S(1)}, u32[]{:S(2)}, u32[]{:S(2)}) collective-permute-start(bf16[192,256]{1,0:T(8,128)(2,1)S(1)} %collective-permute-done.2), channel_id=1, source_target_pairs={{0,2},{2,4},{4,6},{6,8},{8,10},{10,12},{12,14},{14,16},{16,18},{18... | collective-permute-start | bytes 294920 | tf_op jit(solution)/shard_map/ppermute | solution.py:67
  41.7 7.4 %collective-permute-start.4 = (bf16[192,256]{1,0:T(8,128)(2,1)S(1)}, bf16[192,256]{1,0:T(8,128)(2,1)S(1)}, u32[]{:S(2)}, u32[]{:S(2)}) collective-permute-start(bf16[192,256]{1,0:T(8,128)(2,1)S(1)} %collective-permute-done.3), channel_id=1, source_target_pairs={{0,2},{2,4},{4,6},{6,8},{8,10},{10,12},{12,14},{14,16},{16,18},{18... | collective-permute-start | bytes 294920 | tf_op jit(solution)/shard_map/ppermute | solution.py:67
  49.1 6.7 %collective-permute-start.5 = (bf16[192,256]{1,0:T(8,128)(2,1)S(1)}, bf16[192,256]{1,0:T(8,128)(2,1)S(1)}, u32[]{:S(2)}, u32[]{:S(2)}) collective-permute-start(bf16[192,256]{1,0:T(8,128)(2,1)S(1)} %collective-permute-done.4), channel_id=1, source_target_pairs={{0,2},{2,4},{4,6},{6,8},{8,10},{10,12},{12,14},{14,16},{16,18},{18... | collective-permute-start | bytes 294920 | tf_op jit(solution)/shard_map/ppermute | solution.py:67
  55.8 6.7 %collective-permute-start.6 = (bf16[192,256]{1,0:T(8,128)(2,1)S(1)}, bf16[192,256]{1,0:T(8,128)(2,1)S(1)}, u32[]{:S(2)}, u32[]{:S(2)}) collective-permute-start(bf16[192,256]{1,0:T(8,128)(2,1)S(1)} %collective-permute-done.5), channel_id=1, source_target_pairs={{0,2},{2,4},{4,6},{6,8},{8,10},{10,12},{12,14},{14,16},{16,18},{18... | collective-permute-start | bytes 294920 | tf_op jit(solution)/shard_map/ppermute | solution.py:67
  62.6 6.7 %collective-permute-start.7 = (bf16[192,256]{1,0:T(8,128)(2,1)S(1)}, bf16[192,256]{1,0:T(8,128)(2,1)S(1)}, u32[]{:S(2)}, u32[]{:S(2)}) collective-permute-start(bf16[192,256]{1,0:T(8,128)(2,1)S(1)} %collective-permute-done.6), channel_id=1, source_target_pairs={{0,2},{2,4},{4,6},{6,8},{8,10},{10,12},{12,14},{14,16},{16,18},{18... | collective-permute-start | bytes 294920 | tf_op jit(solution)/shard_map/ppermute | solution.py:67
  69.3 6.7 %collective-permute-start.8 = (bf16[192,256]{1,0:T(8,128)(2,1)S(1)}, bf16[192,256]{1,0:T(8,128)(2,1)S(1)}, u32[]{:S(2)}, u32[]{:S(2)}) collective-permute-start(bf16[192,256]{1,0:T(8,128)(2,1)S(1)} %collective-permute-done.7), channel_id=1, source_target_pairs={{0,2},{2,4},{4,6},{6,8},{8,10},{10,12},{12,14},{14,16},{16,18},{18... | collective-permute-start | bytes 294920 | tf_op jit(solution)/shard_map/ppermute | solution.py:67
  76.1 6.7 %collective-permute-start.9 = (bf16[192,256]{1,0:T(8,128)(2,1)S(1)}, bf16[192,256]{1,0:T(8,128)(2,1)S(1)}, u32[]{:S(2)}, u32[]{:S(2)}) collective-permute-start(bf16[192,256]{1,0:T(8,128)(2,1)S(1)} %collective-permute-done.8), channel_id=1, source_target_pairs={{0,2},{2,4},{4,6},{6,8},{8,10},{10,12},{12,14},{14,16},{16,18},{18... | collective-permute-start | bytes 294920 | tf_op jit(solution)/shard_map/ppermute | solution.py:67
  82.8 6.7 %collective-permute-start.10 = (bf16[192,256]{1,0:T(8,128)(2,1)S(1)}, bf16[192,256]{1,0:T(8,128)(2,1)S(1)}, u32[]{:S(2)}, u32[]{:S(2)}) collective-permute-start(bf16[192,256]{1,0:T(8,128)(2,1)S(1)} %collective-permute-done.9), channel_id=1, source_target_pairs={{0,2},{2,4},{4,6},{6,8},{8,10},{10,12},{12,14},{14,16},{16,18},{18... | collective-permute-start | bytes 294920 | tf_op jit(solution)/shard_map/ppermute | solution.py:67
  89.5 6.7 %collective-permute-start.11 = (bf16[192,256]{1,0:T(8,128)(2,1)S(1)}, bf16[192,256]{1,0:T(8,128)(2,1)S(1)}, u32[]{:S(2)}, u32[]{:S(2)}) collective-permute-start(bf16[192,256]{1,0:T(8,128)(2,1)S(1)} %collective-permute-done.10), channel_id=1, source_target_pairs={{0,2},{2,4},{4,6},{6,8},{8,10},{10,12},{12,14},{14,16},{16,18},{18... | collective-permute-start | bytes 294920 | tf_op jit(solution)/shard_map/ppermute | solution.py:67
  96.3 6.7 %collective-permute-start.12 = (bf16[192,256]{1,0:T(8,128)(2,1)S(1)}, bf16[192,256]{1,0:T(8,128)(2,1)S(1)}, u32[]{:S(2)}, u32[]{:S(2)}) collective-permute-start(bf16[192,256]{1,0:T(8,128)(2,1)S(1)} %collective-permute-done.11), channel_id=1, source_target_pairs={{0,2},{2,4},{4,6},{6,8},{8,10},{10,12},{12,14},{14,16},{16,18},{18... | collective-permute-start | bytes 294920 | tf_op jit(solution)/shard_map/ppermute | solution.py:67
  103.0 6.7 %collective-permute-start.13 = (bf16[192,256]{1,0:T(8,128)(2,1)S(1)}, bf16[192,256]{1,0:T(8,128)(2,1)S(1)}, u32[]{:S(2)}, u32[]{:S(2)}) collective-permute-start(bf16[192,256]{1,0:T(8,128)(2,1)S(1)} %collective-permute-done.12), channel_id=1, source_target_pairs={{0,2},{2,4},{4,6},{6,8},{8,10},{10,12},{12,14},{14,16},{16,18},{18... | collective-permute-start | bytes 294920 | tf_op jit(solution)/shard_map/ppermute | solution.py:67
  109.8 6.7 %collective-permute-start.14 = (bf16[192,256]{1,0:T(8,128)(2,1)S(1)}, bf16[192,256]{1,0:T(8,128)(2,1)S(1)}, u32[]{:S(2)}, u32[]{:S(2)}) collective-permute-start(bf16[192,256]{1,0:T(8,128)(2,1)S(1)} %collective-permute-done.13), channel_id=1, source_target_pairs={{0,2},{2,4},{4,6},{6,8},{8,10},{10,12},{12,14},{14,16},{16,18},{18... | collective-permute-start | bytes 294920 | tf_op jit(solution)/shard_map/ppermute | solution.py:67
  136.2 1.0 copy-start
  139.1 0.8 copy-start.1
  141.5 1.0 copy-start
  144.4 0.8 copy-start.1
  146.9 1.0 copy-start
  149.7 0.8 copy-start.1
  152.2 1.2 copy-start
  155.3 0.8 copy-start.1
  157.8 1.0 copy-start
  160.6 0.8 copy-start.1
  163.1 1.0 copy-start
  166.0 0.8 copy-start.1
  168.2 10.9 %copy-start.4 = (f32[2048]{0:T(1024)S(1)}, f32[2048]{0:T(1024)}, u32[]{:S(2)}) copy-start(f32[2048]{0:T(1024)} %param.20) | copy-start | bytes 24580
Sparse Core Ops, SparseCore 0:
  9.6 43.5 all-gather.5
  54.8 55.5 all-gather.7
  112.7 93.9 all-gather.9
  208.8 92.2 all-gather.11
  303.1 95.1 all-gather.13
  412.2 15.6 reduce-scatter.1
